TPU v7x, 32 devices: a whole 2x2x4 slice. The times are simulated.
32 devices in a mesh: grp: 2 (over y), ra: 4 (over z), cb: 4 (over x, core).
Axes of the slice: x: 2, y: 2, z: 4, core: 2. Of those that a mesh axis runs over, the one named last changes fastest.
Arguments:
- tokens: bfloat16 [256, 2048], P('grp', 'ra'), parts along dimension 0, may hold values from -8 to 8
- first_gain: bfloat16 [2048], P('ra'), may hold values from 0.099609375 to 1.8984375
- first_gate: bfloat16 [2048, 5632], P('ra', 'cb'), may hold values from -0.125 to 0.125
- first_up: bfloat16 [2048, 5632], P('ra', 'cb'), may hold values from -0.125 to 0.125
- first_down: bfloat16 [5632, 2048], P('cb', 'ra'), may hold values from -0.078125 to 0.078125
- second_gain: bfloat16 [2048], P('ra'), may hold values from 0.099609375 to 1.8984375
- second_gate: bfloat16 [2048, 5632], P('ra', 'cb'), may hold values from -0.125 to 0.125
- second_up: bfloat16 [2048, 5632], P('ra', 'cb'), may hold values from -0.125 to 0.125
- second_down: bfloat16 [5632, 2048], P('cb', 'ra'), may hold values from -0.078125 to 0.078125
Outputs:
- latent_out: bfloat16 [256, 2048], P('grp', 'ra'), parts along dimension 0
There are 2 independent parts, one for each index of `grp`. A program takes and returns all parts, laid end to end along the dimension named above; an argument that names none is the same for every part. Nothing has to cross between parts.
All inputs are finite; a program needn't handle non-finite values.
Results may differ from a plain program's by a relative error of at most 0.0088.
Values may be sent and summed in bfloat16 or wider, within the bound.
No kernel may reach another device: no remote copies, remote signals or barrier semaphores. Data moves between devices by JAX's collectives and lax.ppermute only.
A program may use at most 64 MiB of HBM per device.

v0:
```python
import jax
import jax.numpy as jnp
from jax import lax
from jax.sharding import PartitionSpec as P


def sublayer(x, gain, w_gate, w_up, w_down):
    xf = x.astype(jnp.float32)
    width = x.shape[1] * lax.axis_size("ra")
    rows = x.shape[0]
    squares = jnp.sum(xf * xf, axis=1)
    normed = (xf * gain.astype(jnp.float32)).astype(jnp.bfloat16)
    dims = (((0,), (1,)), ((), ()))
    gate_rows = lax.dot_general(w_gate, normed, dims, preferred_element_type=jnp.float32)
    up_rows = lax.dot_general(w_up, normed, dims, preferred_element_type=jnp.float32)
    shares = lax.psum_scatter(
        jnp.concatenate([gate_rows, up_rows], axis=1), "ra", scatter_dimension=0, tiled=True
    )
    total_sq = lax.psum(squares, "ra")
    scale = lax.rsqrt(total_sq / width + 1e-06)
    hidden_t = (
        jax.nn.silu(shares[:, :rows] * scale[None, :]) * (shares[:, rows:] * scale[None, :])
    ).astype(jnp.bfloat16)
    partial_value = lax.dot_general(
        lax.all_gather(hidden_t, "ra", axis=0, tiled=True),
        w_down,
        (((0,), (0,)), ((), ())),
        preferred_element_type=jnp.float32,
    )
    branch = lax.psum(partial_value, "cb")
    return (0.5 * xf + 0.5 * branch).astype(jnp.bfloat16)


def per_device(
    tokens,
    first_gain,
    first_gate,
    first_up,
    first_down,
    second_gain,
    second_gate,
    second_up,
    second_down,
):
    middle = sublayer(tokens, first_gain, first_gate, first_up, first_down)
    return sublayer(middle, second_gain, second_gate, second_up, second_down)


def solution(mesh):
    placed = (
        P("grp", "ra"),
        P("ra"),
        P("ra", "cb"),
        P("ra", "cb"),
        P("cb", "ra"),
        P("ra"),
        P("ra", "cb"),
        P("ra", "cb"),
        P("cb", "ra"),
    )
    return jax.shard_map(
        per_device, mesh=mesh, in_specs=placed, out_specs=P("grp", "ra"), check_vma=False
    )
```

profile of v0, /device:TPU:0, one launch (start us, length us, event | category | flops | bytes accessed | tf_op | source)
XLA Modules:
  0.0 194.4 jit_solution(9216063514448310554)
XLA Ops:
  6.5 0.8 convert_element_type.31
  7.4 0.5 copy-done
  7.9 1.3 convolution_bitcast_fusion.2
  9.2 0.4 convolution_bitcast_fusion.3
  9.7 1.6 copy.12
  11.5 13.6 %psum.28 = f32[128]{0:T(128)S(1)} all-reduce(f32[128]{0:T(128)S(1)} %fusion.1), channel_id=1, replica_groups=mesh['grp'=2,'ra'=4,'cb'=4] {'ra'}, use_global_device_ids=true, to_apply=%region_2.0 | all-reduce | flops 128 | bytes 1024 | tf_op jit(solution)/shard_map/psum | solution.py:19
  25.1 22.5 %reduce-scatter.7.cloned.1.call-done = f32[352,256]{1,0:T(8,128)} async-done(((f32[1408,256]{1,0:T(8,128)}), f32[352,256]{1,0:T(8,128)}) %reduce-scatter.7.cloned.1.call-update) | async-done | bytes 360464
  47.6 1.7 fusion.14
  49.4 1.1 copy.17
  50.8 15.0 %all_gather.6 = bf16[1408,128]{1,0:T(8,128)(2,1)S(1)} all-gather(bf16[352,128]{1,0:T(8,128)(2,1)S(1)} %copy.10), channel_id=1, replica_groups=mesh['grp'=2,'ra'=4,'cb'=4] {'ra'}, dimensions={0}, use_global_device_ids=true | all-gather | bytes 450560 | tf_op jit(solution)/shard_map/all_gather | solution.py:25
  65.8 1.1 fusion.15
  67.0 30.7 %all-reduce.3.cloned.1.call-done = f32[128,512]{1,0:T(8,128)} async-done(((f32[128,512]{1,0:T(8,128)}), f32[128,512]{1,0:T(8,128)}) %all-reduce.3.cloned.1.call-update) | async-done | bytes 262160 | tf_op jit(solution)/shard_map/psum | solution.py:30
  97.7 1.1 fusion.5
  98.8 1.7 convolution_bitcast_fusion
  100.5 0.4 convolution_bitcast_fusion.1
  101.0 1.6 copy.14
  102.6 12.1 %psum.30 = f32[128]{0:T(128)S(1)} all-reduce(f32[128]{0:T(128)S(1)} %get-tuple-element.5), channel_id=1, replica_groups=mesh['grp'=2,'ra'=4,'cb'=4] {'ra'}, use_global_device_ids=true, to_apply=%region_6.7 | all-reduce | flops 128 | bytes 1024 | tf_op jit(solution)/shard_map/psum | solution.py:19
  114.7 21.5 %reduce-scatter.9.cloned.1.call-done = f32[352,256]{1,0:T(8,128)} async-done(((f32[1408,256]{1,0:T(8,128)}), f32[352,256]{1,0:T(8,128)}) %reduce-scatter.9.cloned.1.call-update) | async-done | bytes 360464
  136.2 1.7 fusion.13
  138.0 1.1 copy.19
  139.3 15.1 %all_gather.7 = bf16[1408,128]{1,0:T(8,128)(2,1)S(1)} all-gather(bf16[352,128]{1,0:T(8,128)(2,1)S(1)} %copy.11), channel_id=1, replica_groups=mesh['grp'=2,'ra'=4,'cb'=4] {'ra'}, dimensions={0}, use_global_device_ids=true | all-gather | bytes 450560 | tf_op jit(solution)/shard_map/all_gather | solution.py:25
  154.4 1.1 fusion.16
  155.5 30.7 %all-reduce.5.cloned.1.call-done = f32[128,512]{1,0:T(8,128)} async-done(((f32[128,512]{1,0:T(8,128)}), f32[128,512]{1,0:T(8,128)}) %all-reduce.5.cloned.1.call-update) | async-done | bytes 262160 | tf_op jit(solution)/shard_map/psum | solution.py:30
  186.2 1.6 fusion.7
  (33 shorter events, 1.3 us)
Async XLA Ops:
  6.5 1.4 copy-start
  6.5 2.7 %copy-start.1 = (bf16[128,512]{1,0:T(8,128)(2,1)S(1)}, bf16[128,512]{1,0:T(8,128)(2,1)}, u32[]{:S(2)}) copy-start(bf16[128,512]{1,0:T(8,128)(2,1)} %param.9) | copy-start | bytes 393220
  6.5 2.7 %copy-start.2 = (bf16[512,1408]{1,0:T(8,128)(2,1)S(1)}, bf16[512,1408]{1,0:T(8,128)(2,1)}, u32[]{:S(2)}) copy-start(bf16[512,1408]{1,0:T(8,128)(2,1)} %param.11) | copy-start | bytes 4325380
  6.5 41.1 %reduce-scatter.7.cloned.1.call-start = ((), (), s32[]{:S(2)}) async-start(), calls=%async_computation.4 | async-start | bytes 1802240
  11.3 54.5 %copy-start.3 = (bf16[1408,512]{1,0:T(8,128)(2,1)S(1)}, bf16[1408,512]{1,0:T(8,128)(2,1)}, u32[]{:S(2)}) copy-start(bf16[1408,512]{1,0:T(8,128)(2,1)} %param.13) | copy-start | bytes 4325380
  11.3 86.4 %all-reduce.3.cloned.1.call-start = ((), (), s32[]{:S(2)}) async-start(), calls=%async_computation.2 | async-start | bytes 524288 | tf_op jit(solution)/shard_map/psum | solution.py:30
  50.6 16.3 %copy-start.6 = (bf16[512]{0:T(512)(128)(2,1)S(1)}, bf16[512]{0:T(512)(128)(2,1)}, u32[]{:S(2)}) copy-start(bf16[512]{0:T(512)(128)(2,1)} %param.14) | copy-start | bytes 3076
  66.9 33.6 %copy-start.4 = (bf16[512,1408]{1,0:T(8,128)(2,1)S(1)}, bf16[512,1408]{1,0:T(8,128)(2,1)}, u32[]{:S(2)}) copy-start(bf16[512,1408]{1,0:T(8,128)(2,1)} %param.15) | copy-start | bytes 4325380
  66.9 69.3 %reduce-scatter.9.cloned.1.call-start = ((), (), s32[]{:S(2)}) async-start(), calls=%async_computation.5 | async-start | bytes 1802240
  102.6 51.8 %copy-start.5 = (bf16[1408,512]{1,0:T(8,128)(2,1)S(1)}, bf16[1408,512]{1,0:T(8,128)(2,1)}, u32[]{:S(2)}) copy-start(bf16[1408,512]{1,0:T(8,128)(2,1)} %param.17) | copy-start | bytes 4325380
  102.6 83.6 %all-reduce.5.cloned.1.call-start = ((), (), s32[]{:S(2)}) async-start(), calls=%async_computation.3 | async-start | bytes 524288 | tf_op jit(solution)/shard_map/psum | solution.py:30
Sparse Core Ops, SparseCore 0:
  11.4 36.1 reduce-scatter.6
  67.0 30.5 all-reduce.2
  102.7 33.4 reduce-scatter.8
  155.7 30.5 all-reduce.4
where the time goes:
time: 195 us; the launch traced here: 194 us
  waiting for transfers between devices  105 us (54%)
  blocking collectives  55.8 us (29%)
  between operations  13.3 us (7%)
  local copies, waits for them, and re-layouts  9.67 us (5%)
  matrix products  6.01 us (3%)
  other arithmetic  4.14 us (2%)
    psum x2, waiting for transfers between devices, sublayer(): branch = lax.psum(partial_value, 'cb')  61.4 us
    unnamed x6, waiting for transfers between devices  44 us
    all_gather x2, blocking collectives, sublayer(): lax.all_gather(hidden_t, 'ra', axis=0, tiled=True)  30.1 us
    psum x2, blocking collectives, sublayer(): total_sq = lax.psum(squares, 'ra')  25.7 us
    unnamed x20, local copies, waits for them, and re-layouts  6.04 us
  transfers between devices with their start and end apart: 4, of which 4 were waited for; matrix products, arithmetic and copies ran while one was open for 0% of the time, Pallas kernels for 0%

commit v1 on v0

v1 whole, which is shorter than its diff:
```python
import jax
import jax.numpy as jnp
from jax import lax
from jax.sharding import PartitionSpec as P

CHUNKS = 1
bf16, f32 = jnp.bfloat16, jnp.float32


def bits_of(axis):
    size, out, k = lax.axis_size(axis), [], 1
    while k < size:
        out.append(k)
        k *= 2
    assert k == size
    return out


def swap(x, axis, bit):
    return lax.ppermute(x, axis, [(i, i ^ bit) for i in range(lax.axis_size(axis))])


def local_order(x, axis):
    me, levels = lax.axis_index(axis), bits_of(axis)
    y = x.reshape((2,) * len(levels) + (-1, x.shape[1]))
    for dim, bit in enumerate(levels):
        y = jnp.where((me & bit) != 0, jnp.flip(y, dim), y)
    return y.reshape(x.shape)


def up_half(x, gain, w_gate, w_up):
    xf = x.astype(f32)
    squares = jnp.sum(xf * xf, axis=1, keepdims=True)
    high = squares.astype(bf16).astype(f32)
    normed = (xf * gain.astype(f32)).astype(bf16)
    gate = jnp.dot(normed, w_gate, preferred_element_type=f32)
    up = jnp.dot(normed, w_up, preferred_element_type=f32)
    lane = lax.broadcasted_iota(jnp.int32, (x.shape[0], 128), 1)
    sq = jnp.where(lane == 0, high, jnp.where(lane == 1, squares - high, 0.0))
    return jnp.concatenate([gate, up, sq], axis=1)


def sublayer(x, gain, w_gate, w_up, w_down):
    width = x.shape[1] * lax.axis_size("ra")
    ff = w_gate.shape[1]
    part = up_half(x, gain, w_gate, w_up)
    for bit in bits_of("ra"):
        half = part.shape[0] // 2
        part = part[:half] + swap(part[half:].astype(bf16), "ra", bit).astype(f32)
    total = part[:, 2 * ff : 2 * ff + 1] + part[:, 2 * ff + 1 : 2 * ff + 2]
    scale = lax.rsqrt(total / width + 1e-06)
    hidden = (jax.nn.silu(part[:, :ff] * scale) * (part[:, ff : 2 * ff] * scale)).astype(bf16)
    for bit in reversed(bits_of("ra")):
        hidden = jnp.concatenate([hidden, swap(hidden, "ra", bit)], axis=0)
    branch = jnp.dot(hidden, w_down, preferred_element_type=f32)
    for bit in bits_of("cb"):
        branch = branch + swap(branch.astype(bf16), "cb", bit).astype(f32)
    return (0.5 * x.astype(f32) + 0.5 * branch).astype(bf16)


def per_device(tokens, first_gain, first_gate, first_up, first_down, second_gain, second_gate, second_up, second_down):
    rows = tokens.shape[0] // CHUNKS
    outs = []
    for c in range(CHUNKS):
        x = local_order(tokens[c * rows : (c + 1) * rows], "ra")
        x = sublayer(x, first_gain, first_gate, first_up, first_down)
        x = sublayer(x, second_gain, second_gate, second_up, second_down)
        outs.append(local_order(x, "ra"))
    return jnp.concatenate(outs, axis=0)


def solution(mesh):
    placed = (
        P("grp", "ra"),
        P("ra"),
        P("ra", "cb"),
        P("ra", "cb"),
        P("cb", "ra"),
        P("ra"),
        P("ra", "cb"),
        P("ra", "cb"),
        P("cb", "ra"),
    )
    return jax.shard_map(
        per_device, mesh=mesh, in_specs=placed, out_specs=P("grp", "ra"), check_vma=False
    )
```

time: 195 us -> 89.2 us (0.46)
  blocking collectives: 55.8 us -> 0 us
  waiting for transfers between devices: 105 us -> 71.6 us
  between operations: 13.3 us -> 0.29 us
  starting transfers between devices: 0.13 us -> 10.3 us
  local copies, waits for them, and re-layouts: 9.67 us -> 0.25 us
  matrix products: 6.01 us -> 2.27 us
    ppermute x0 -> x12, waiting for transfers between devices: none -> 71.6 us  [swap(): lax.ppermute(x, axis, [(i, i ^ bit) for i in range(lax.axis_size(axis))])]
    psum x2 -> x0, waiting for transfers between devices: 61.4 us -> none  [sublayer(): branch = lax.psum(partial_value, 'cb')]
    unnamed x6 -> x0, waiting for transfers between devices: 44 us -> none
    all_gather x2 -> x0, blocking collectives: 30.1 us -> none  [sublayer(): lax.all_gather(hidden_t, 'ra', axis=0, tiled=True)]
    psum x2 -> x0, blocking collectives: 25.7 us -> none  [sublayer(): total_sq = lax.psum(squares, 'ra')]
    ppermute x0 -> x12, starting transfers between devices: none -> 10.3 us  [swap(): lax.ppermute(x, axis, [(i, i ^ bit) for i in range(lax.axis_size(axis))])]
    unnamed x20 -> x14, local copies, waits for them, and re-layouts: 6.04 us -> 0.04 us
    dot_general x6, matrix products: 6.01 us -> 2.27 us  [the longest x2 0.76 us: up_half(): up = jnp.dot(normed, w_up, preferred_element_type=f32)]
  transfers between devices with their start and end apart: 4 -> 12, of which waited for: 4 -> 12; matrix products, arithmetic and copies ran while one was open for 0% -> 0% of each run, Pallas kernels for 0% -> 0%
where the time goes in v1:
time: 89.2 us; the launch traced here: 89 us
  waiting for transfers between devices  71.6 us (80%)
  starting transfers between devices  10.3 us (12%)
  other arithmetic  4.37 us (5%)
  matrix products  2.27 us (3%)
    ppermute x12, waiting for transfers between devices, swap(): lax.ppermute(x, axis, [(i, i ^ bit) for i in range(lax.axis_size(axis))])  71.6 us
    ppermute x12, starting transfers between devices, swap(): lax.ppermute(x, axis, [(i, i ^ bit) for i in range(lax.axis_size(axis))])  10.3 us
    select_n x3, other arithmetic, local_order(): y = jnp.where(me & bit != 0, jnp.flip(y, dim), y)  1.87 us
  transfers between devices with their start and end apart: 12, of which 12 were waited for; matrix products, arithmetic and copies ran while one was open for 0% of the time, Pallas kernels for 0%

profile of v1, /device:TPU:0, one launch (start us, length us, event | category | flops | bytes accessed | tf_op | source)
XLA Modules:
  0.0 89.0 jit_solution(13418669889279714464)
XLA Ops:
  0.0 1.2 %reverse_select_fusion.3 = bf16[2,2,32,512]{3,2,1,0:T(8,128)(2,1)S(1)} fusion(bf16[2,2,32,512]{3,2,1,0:T(8,128)(2,1)} %bitcast.22, pred[]{:T(512)S(6)} %ne.9), kind=kLoop, calls=%fused_computation.41 | loop fusion | flops 65536 | bytes 262145 | tf_op jit(solution)/shard_map/jit(_where)/select_n | solution.py:27
  1.4 0.7 convert_element_type.124
  2.1 0.4 fusion.45
  2.5 0.4 fusion.46
  3.2 3.1 %collective-permute-start = (bf16[64,2944]{1,0:T(8,128)(2,1)S(1)}, bf16[64,2944]{1,0:T(8,128)(2,1)S(1)}, u32[]{:S(2)}, u32[]{:S(2)}) collective-permute-start(bf16[64,2944]{1,0:T(8,128)(2,1)S(1)} %slice.129), channel_id=1, source_target_pairs={{0,4},{4,0},{8,12},{12,8},{1,5},{5,1},{9,13},{13,9},{2,6},{6,2},{1... | collective-permute-start | bytes 1130504 | tf_op jit(solution)/shard_map/ppermute | solution.py:20
  6.3 8.8 %collective-permute-done = bf16[64,2944]{1,0:T(8,128)(2,1)S(1)} collective-permute-done((bf16[64,2944]{1,0:T(8,128)(2,1)S(1)}, bf16[64,2944]{1,0:T(8,128)(2,1)S(1)}, u32[]{:S(2)}, u32[]{:S(2)}) %collective-permute-start) | collective-permute-done | bytes 376864 | tf_op jit(solution)/shard_map/ppermute | solution.py:20
  15.2 2.8 %collective-permute-start.1 = (bf16[32,2944]{1,0:T(8,128)(2,1)S(1)}, bf16[32,2944]{1,0:T(8,128)(2,1)S(1)}, u32[]{:S(2)}, u32[]{:S(2)}) collective-permute-start(bf16[32,2944]{1,0:T(8,128)(2,1)S(1)} %slice.131), channel_id=1, source_target_pairs={{0,8},{4,12},{8,0},{12,4},{1,9},{5,13},{9,1},{13,5},{2,10},{6,14},... | collective-permute-start | bytes 565256 | tf_op jit(solution)/shard_map/ppermute | solution.py:20
  18.0 8.1 %collective-permute-done.1 = bf16[32,2944]{1,0:T(8,128)(2,1)S(1)} collective-permute-done((bf16[32,2944]{1,0:T(8,128)(2,1)S(1)}, bf16[32,2944]{1,0:T(8,128)(2,1)S(1)}, u32[]{:S(2)}, u32[]{:S(2)}) %collective-permute-start.1) | collective-permute-done | bytes 188448 | tf_op jit(solution)/shard_map/ppermute | solution.py:20
  26.6 7.1 %collective-permute-done.2 = bf16[32,1408]{1,0:T(8,128)(2,1)S(1)} collective-permute-done((bf16[32,1408]{1,0:T(8,128)(2,1)S(1)}, bf16[32,1408]{1,0:T(8,128)(2,1)S(1)}, u32[]{:S(2)}, u32[]{:S(2)}) %collective-permute-start.2) | collective-permute-done | bytes 90144 | tf_op jit(solution)/shard_map/ppermute | solution.py:20
  33.8 5.5 %collective-permute-done.3 = bf16[64,1408]{1,0:T(8,128)(2,1)S(1)} collective-permute-done((bf16[64,1408]{1,0:T(8,128)(2,1)S(1)}, bf16[64,1408]{1,0:T(8,128)(2,1)S(1)}, u32[]{:S(2)}, u32[]{:S(2)}) %collective-permute-start.3) | collective-permute-done | bytes 180256 | tf_op jit(solution)/shard_map/ppermute | solution.py:20
  39.7 1.3 %collective-permute-done.4 = bf16[128,512]{1,0:T(8,128)(2,1)S(1)} collective-permute-done((bf16[128,512]{1,0:T(8,128)(2,1)S(1)}, bf16[128,512]{1,0:T(8,128)(2,1)S(1)}, u32[]{:S(2)}, u32[]{:S(2)}) %collective-permute-start.4) | collective-permute-done | bytes 131104 | tf_op jit(solution)/shard_map/ppermute | solution.py:20
  41.1 1.6 %collective-permute-start.5 = (bf16[128,512]{1,0:T(8,128)(2,1)S(1)}, bf16[128,512]{1,0:T(8,128)(2,1)S(1)}, u32[]{:S(2)}, u32[]{:S(2)}) collective-permute-start(bf16[128,512]{1,0:T(8,128)(2,1)S(1)} %fusion.20), channel_id=1, source_target_pairs={{0,2},{1,3},{2,0},{3,1},{4,6},{5,7},{6,4},{7,5},{8,10},{9,11},{10,... | collective-permute-start | bytes 393224 | tf_op jit(solution)/shard_map/ppermute | solution.py:20
  42.7 4.0 %collective-permute-done.5 = bf16[128,512]{1,0:T(8,128)(2,1)S(1)} collective-permute-done((bf16[128,512]{1,0:T(8,128)(2,1)S(1)}, bf16[128,512]{1,0:T(8,128)(2,1)S(1)}, u32[]{:S(2)}, u32[]{:S(2)}) %collective-permute-start.5) | collective-permute-done | bytes 131104 | tf_op jit(solution)/shard_map/ppermute | solution.py:20
  47.3 0.4 fusion.28
  48.0 10.0 %collective-permute-done.6 = bf16[64,2944]{1,0:T(8,128)(2,1)S(1)} collective-permute-done((bf16[64,2944]{1,0:T(8,128)(2,1)S(1)}, bf16[64,2944]{1,0:T(8,128)(2,1)S(1)}, u32[]{:S(2)}, u32[]{:S(2)}) %collective-permute-start.6) | collective-permute-done | bytes 376864 | tf_op jit(solution)/shard_map/ppermute | solution.py:20
  58.1 0.7 collective-permute-start.7
  58.8 9.4 %collective-permute-done.7 = bf16[32,2944]{1,0:T(8,128)(2,1)S(1)} collective-permute-done((bf16[32,2944]{1,0:T(8,128)(2,1)S(1)}, bf16[32,2944]{1,0:T(8,128)(2,1)S(1)}, u32[]{:S(2)}, u32[]{:S(2)}) %collective-permute-start.7) | collective-permute-done | bytes 188448 | tf_op jit(solution)/shard_map/ppermute | solution.py:20
  68.6 5.9 %collective-permute-done.8 = bf16[32,1408]{1,0:T(8,128)(2,1)S(1)} collective-permute-done((bf16[32,1408]{1,0:T(8,128)(2,1)S(1)}, bf16[32,1408]{1,0:T(8,128)(2,1)S(1)}, u32[]{:S(2)}, u32[]{:S(2)}) %collective-permute-start.8) | collective-permute-done | bytes 90144 | tf_op jit(solution)/shard_map/ppermute | solution.py:20
  74.7 6.1 %collective-permute-done.9 = bf16[64,1408]{1,0:T(8,128)(2,1)S(1)} collective-permute-done((bf16[64,1408]{1,0:T(8,128)(2,1)S(1)}, bf16[64,1408]{1,0:T(8,128)(2,1)S(1)}, u32[]{:S(2)}, u32[]{:S(2)}) %collective-permute-start.9) | collective-permute-done | bytes 180256 | tf_op jit(solution)/shard_map/ppermute | solution.py:20
  80.8 0.4 fusion.44
  81.2 1.3 %collective-permute-done.10 = bf16[128,512]{1,0:T(8,128)(2,1)S(1)} collective-permute-done((bf16[128,512]{1,0:T(8,128)(2,1)S(1)}, bf16[128,512]{1,0:T(8,128)(2,1)S(1)}, u32[]{:S(2)}, u32[]{:S(2)}) %collective-permute-start.10) | collective-permute-done | bytes 131104 | tf_op jit(solution)/shard_map/ppermute | solution.py:20
  82.6 1.6 %collective-permute-start.11 = (bf16[128,512]{1,0:T(8,128)(2,1)S(1)}, bf16[128,512]{1,0:T(8,128)(2,1)S(1)}, u32[]{:S(2)}, u32[]{:S(2)}) collective-permute-start(bf16[128,512]{1,0:T(8,128)(2,1)S(1)} %fusion.21), channel_id=1, source_target_pairs={{0,2},{1,3},{2,0},{3,1},{4,6},{5,7},{6,4},{7,5},{8,10},{9,11},{10,... | collective-permute-start | bytes 393224 | tf_op jit(solution)/shard_map/ppermute | solution.py:20
  84.2 4.0 %collective-permute-done.11 = bf16[128,512]{1,0:T(8,128)(2,1)S(1)} collective-permute-done((bf16[128,512]{1,0:T(8,128)(2,1)S(1)}, bf16[128,512]{1,0:T(8,128)(2,1)S(1)}, u32[]{:S(2)}, u32[]{:S(2)}) %collective-permute-start.11) | collective-permute-done | bytes 131104 | tf_op jit(solution)/shard_map/ppermute | solution.py:20
  88.4 0.7 reverse_select_fusion
  (53 shorter events, 3.3 us)
Async XLA Ops:
  0.0 2.1 %copy-start = (bf16[512,1408]{1,0:T(8,128)(2,1)S(1)}, bf16[512,1408]{1,0:T(8,128)(2,1)}, u32[]{:S(2)}) copy-start(bf16[512,1408]{1,0:T(8,128)(2,1)} %param.11) | copy-start | bytes 4325380
  0.0 2.5 %copy-start.1 = (bf16[512,1408]{1,0:T(8,128)(2,1)S(1)}, bf16[512,1408]{1,0:T(8,128)(2,1)}, u32[]{:S(2)}) copy-start(bf16[512,1408]{1,0:T(8,128)(2,1)} %param.12) | copy-start | bytes 4325380
  3.2 11.9 %collective-permute-start = (bf16[64,2944]{1,0:T(8,128)(2,1)S(1)}, bf16[64,2944]{1,0:T(8,128)(2,1)S(1)}, u32[]{:S(2)}, u32[]{:S(2)}) collective-permute-start(bf16[64,2944]{1,0:T(8,128)(2,1)S(1)} %slice.129), channel_id=1, source_target_pairs={{0,4},{4,0},{8,12},{12,8},{1,5},{5,1},{9,13},{13,9},{2,6},{6,2},{1... | collective-permute-start | bytes 1130504 | tf_op jit(solution)/shard_map/ppermute | solution.py:20
  15.2 24.1 %copy-start.5 = (bf16[1408,512]{1,0:T(8,128)(2,1)S(1)}, bf16[1408,512]{1,0:T(8,128)(2,1)}, u32[]{:S(2)}) copy-start(bf16[1408,512]{1,0:T(8,128)(2,1)} %param.13) | copy-start | bytes 4325380
  15.2 10.9 %collective-permute-start.1 = (bf16[32,2944]{1,0:T(8,128)(2,1)S(1)}, bf16[32,2944]{1,0:T(8,128)(2,1)S(1)}, u32[]{:S(2)}, u32[]{:S(2)}) collective-permute-start(bf16[32,2944]{1,0:T(8,128)(2,1)S(1)} %slice.131), channel_id=1, source_target_pairs={{0,8},{4,12},{8,0},{12,4},{1,9},{5,13},{9,1},{13,5},{2,10},{6,14},... | collective-permute-start | bytes 565256 | tf_op jit(solution)/shard_map/ppermute | solution.py:20
  26.5 7.2 %collective-permute-start.2 = (bf16[32,1408]{1,0:T(8,128)(2,1)S(1)}, bf16[32,1408]{1,0:T(8,128)(2,1)S(1)}, u32[]{:S(2)}, u32[]{:S(2)}) collective-permute-start(bf16[32,1408]{1,0:T(8,128)(2,1)S(1)} %fusion.25), channel_id=1, source_target_pairs={{0,8},{4,12},{8,0},{12,4},{1,9},{5,13},{9,1},{13,5},{2,10},{6,14},... | collective-permute-start | bytes 270344 | tf_op jit(solution)/shard_map/ppermute | solution.py:20
  33.7 9.0 %copy-start.4 = (bf16[512]{0:T(512)(128)(2,1)S(1)}, bf16[512]{0:T(512)(128)(2,1)}, u32[]{:S(2)}) copy-start(bf16[512]{0:T(512)(128)(2,1)} %param.14) | copy-start | bytes 3076
  33.7 13.2 %copy-start.2 = (bf16[512,1408]{1,0:T(8,128)(2,1)S(1)}, bf16[512,1408]{1,0:T(8,128)(2,1)}, u32[]{:S(2)}) copy-start(bf16[512,1408]{1,0:T(8,128)(2,1)} %param.16) | copy-start | bytes 4325380
  33.7 5.6 %collective-permute-start.3 = (bf16[64,1408]{1,0:T(8,128)(2,1)S(1)}, bf16[64,1408]{1,0:T(8,128)(2,1)S(1)}, u32[]{:S(2)}, u32[]{:S(2)}) collective-permute-start(bf16[64,1408]{1,0:T(8,128)(2,1)S(1)} %pad_maximum_fusion.2), channel_id=1, source_target_pairs={{0,4},{4,0},{8,12},{12,8},{1,5},{5,1},{9,13},{13,9},{2,6},{6,2},{1... | collective-permute-start | bytes 540680 | tf_op jit(solution)/shard_map/ppermute | solution.py:20
  39.7 1.4 %collective-permute-start.4 = (bf16[128,512]{1,0:T(8,128)(2,1)S(1)}, bf16[128,512]{1,0:T(8,128)(2,1)S(1)}, u32[]{:S(2)}, u32[]{:S(2)}) collective-permute-start(bf16[128,512]{1,0:T(8,128)(2,1)S(1)} %get-tuple-element.11), channel_id=1, source_target_pairs={{0,1},{1,0},{2,3},{3,2},{4,5},{5,4},{6,7},{7,6},{8,9},{9,8},{10,11... | collective-permute-start | bytes 393224 | tf_op jit(solution)/shard_map/ppermute | solution.py:20
  41.1 5.6 %collective-permute-start.5 = (bf16[128,512]{1,0:T(8,128)(2,1)S(1)}, bf16[128,512]{1,0:T(8,128)(2,1)S(1)}, u32[]{:S(2)}, u32[]{:S(2)}) collective-permute-start(bf16[128,512]{1,0:T(8,128)(2,1)S(1)} %fusion.20), channel_id=1, source_target_pairs={{0,2},{1,3},{2,0},{3,1},{4,6},{5,7},{6,4},{7,5},{8,10},{9,11},{10,... | collective-permute-start | bytes 393224 | tf_op jit(solution)/shard_map/ppermute | solution.py:20
  42.7 4.6 %copy-start.3 = (bf16[512,1408]{1,0:T(8,128)(2,1)S(1)}, bf16[512,1408]{1,0:T(8,128)(2,1)}, u32[]{:S(2)}) copy-start(bf16[512,1408]{1,0:T(8,128)(2,1)} %param.15) | copy-start | bytes 4325380
  48.0 10.0 %collective-permute-start.6 = (bf16[64,2944]{1,0:T(8,128)(2,1)S(1)}, bf16[64,2944]{1,0:T(8,128)(2,1)S(1)}, u32[]{:S(2)}, u32[]{:S(2)}) collective-permute-start(bf16[64,2944]{1,0:T(8,128)(2,1)S(1)} %slice.128), channel_id=1, source_target_pairs={{0,4},{4,0},{8,12},{12,8},{1,5},{5,1},{9,13},{13,9},{2,6},{6,2},{1... | collective-permute-start | bytes 1130504 | tf_op jit(solution)/shard_map/ppermute | solution.py:20
  58.1 22.7 %copy-start.6 = (bf16[1408,512]{1,0:T(8,128)(2,1)S(1)}, bf16[1408,512]{1,0:T(8,128)(2,1)}, u32[]{:S(2)}) copy-start(bf16[1408,512]{1,0:T(8,128)(2,1)} %param.17) | copy-start | bytes 4325380
  58.1 10.1 %collective-permute-start.7 = (bf16[32,2944]{1,0:T(8,128)(2,1)S(1)}, bf16[32,2944]{1,0:T(8,128)(2,1)S(1)}, u32[]{:S(2)}, u32[]{:S(2)}) collective-permute-start(bf16[32,2944]{1,0:T(8,128)(2,1)S(1)} %slice.130), channel_id=1, source_target_pairs={{0,8},{4,12},{8,0},{12,4},{1,9},{5,13},{9,1},{13,5},{2,10},{6,14},... | collective-permute-start | bytes 565256 | tf_op jit(solution)/shard_map/ppermute | solution.py:20
  68.6 6.0 %collective-permute-start.8 = (bf16[32,1408]{1,0:T(8,128)(2,1)S(1)}, bf16[32,1408]{1,0:T(8,128)(2,1)S(1)}, u32[]{:S(2)}, u32[]{:S(2)}) collective-permute-start(bf16[32,1408]{1,0:T(8,128)(2,1)S(1)} %fusion.23), channel_id=1, source_target_pairs={{0,8},{4,12},{8,0},{12,4},{1,9},{5,13},{9,1},{13,5},{2,10},{6,14},... | collective-permute-start | bytes 270344 | tf_op jit(solution)/shard_map/ppermute | solution.py:20
  74.6 6.2 %collective-permute-start.9 = (bf16[64,1408]{1,0:T(8,128)(2,1)S(1)}, bf16[64,1408]{1,0:T(8,128)(2,1)S(1)}, u32[]{:S(2)}, u32[]{:S(2)}) collective-permute-start(bf16[64,1408]{1,0:T(8,128)(2,1)S(1)} %pad_maximum_fusion.3), channel_id=1, source_target_pairs={{0,4},{4,0},{8,12},{12,8},{1,5},{5,1},{9,13},{13,9},{2,6},{6,2},{1... | collective-permute-start | bytes 540680 | tf_op jit(solution)/shard_map/ppermute | solution.py:20
  81.2 1.4 %collective-permute-start.10 = (bf16[128,512]{1,0:T(8,128)(2,1)S(1)}, bf16[128,512]{1,0:T(8,128)(2,1)S(1)}, u32[]{:S(2)}, u32[]{:S(2)}) collective-permute-start(bf16[128,512]{1,0:T(8,128)(2,1)S(1)} %get-tuple-element.13), channel_id=1, source_target_pairs={{0,1},{1,0},{2,3},{3,2},{4,5},{5,4},{6,7},{7,6},{8,9},{9,8},{10,11... | collective-permute-start | bytes 393224 | tf_op jit(solution)/shard_map/ppermute | solution.py:20
  82.6 5.6 %collective-permute-start.11 = (bf16[128,512]{1,0:T(8,128)(2,1)S(1)}, bf16[128,512]{1,0:T(8,128)(2,1)S(1)}, u32[]{:S(2)}, u32[]{:S(2)}) collective-permute-start(bf16[128,512]{1,0:T(8,128)(2,1)S(1)} %fusion.21), channel_id=1, source_target_pairs={{0,2},{1,3},{2,0},{3,1},{4,6},{5,7},{6,4},{7,5},{8,10},{9,11},{10,... | collective-permute-start | bytes 393224 | tf_op jit(solution)/shard_map/ppermute | solution.py:20

commit v2 on v1

v2 whole, which is shorter than its diff:
```python
import jax
import jax.numpy as jnp
from jax import lax
from jax.sharding import PartitionSpec as P

CHUNKS = 2
bf16, f32 = jnp.bfloat16, jnp.float32


def bits_of(axis):
    size, out, k = lax.axis_size(axis), [], 1
    while k < size:
        out.append(k)
        k *= 2
    assert k == size
    return out


def local_order(x, axis):
    me, levels = lax.axis_index(axis), bits_of(axis)
    y = x.reshape((2,) * len(levels) + (-1, x.shape[1]))
    for dim, bit in enumerate(levels):
        y = jnp.where((me & bit) != 0, jnp.flip(y, dim), y)
    return y.reshape(x.shape)


def up_half(x, gain, w_gate, w_up):
    xf = x.astype(f32)
    squares = jnp.sum(xf * xf, axis=1, keepdims=True)
    high = squares.astype(bf16).astype(f32)
    normed = (xf * gain.astype(f32)).astype(bf16)
    gate = jnp.dot(normed, w_gate, preferred_element_type=f32)
    up = jnp.dot(normed, w_up, preferred_element_type=f32)
    lane = lax.broadcasted_iota(jnp.int32, (x.shape[0], 128), 1)
    sq = jnp.where(lane == 0, high, jnp.where(lane == 1, squares - high, 0.0))
    return jnp.concatenate([gate, up, sq], axis=1)


def chain(x, layers):
    x = local_order(x, "ra")
    for gain, w_gate, w_up, w_down in layers:
        width = x.shape[1] * lax.axis_size("ra")
        ff = w_gate.shape[1]
        part = up_half(x, gain, w_gate, w_up)
        for bit in bits_of("ra"):
            half = part.shape[0] // 2
            got = yield part[half:].astype(bf16), "ra", bit
            part = part[:half] + got.astype(f32)
        total = part[:, 2 * ff : 2 * ff + 1] + part[:, 2 * ff + 1 : 2 * ff + 2]
        scale = lax.rsqrt(total / width + 1e-06)
        hidden = (jax.nn.silu(part[:, :ff] * scale) * (part[:, ff : 2 * ff] * scale)).astype(bf16)
        for bit in reversed(bits_of("ra")):
            got = yield hidden, "ra", bit
            hidden = jnp.concatenate([hidden, got], axis=0)
        branch = jnp.dot(hidden, w_down, preferred_element_type=f32)
        for bit in bits_of("cb"):
            got = yield branch.astype(bf16), "cb", bit
            branch = branch + got.astype(f32)
        x = (0.5 * x.astype(f32) + 0.5 * branch).astype(bf16)
    yield local_order(x, "ra")


def per_device(tokens, first_gain, first_gate, first_up, first_down, second_gain, second_gate, second_up, second_down):
    layers = ((first_gain, first_gate, first_up, first_down), (second_gain, second_gate, second_up, second_down))
    rows = tokens.shape[0] // CHUNKS
    chains = [chain(tokens[c * rows : (c + 1) * rows], layers) for c in range(CHUNKS)]
    arrived, last = [None] * CHUNKS, None
    while True:
        for c in range(CHUNKS):
            asked = chains[c].send(arrived[c])
            if isinstance(asked, tuple):
                payload, axis, bit = asked
                if last is not None:
                    payload, _ = lax.optimization_barrier((payload, last))
                last = payload
                arrived[c] = lax.ppermute(payload, axis, [(i, i ^ bit) for i in range(lax.axis_size(axis))])
            else:
                arrived[c] = asked
        if not isinstance(asked, tuple):
            return jnp.concatenate(arrived, axis=0)


def solution(mesh):
    placed = (
        P("grp", "ra"),
        P("ra"),
        P("ra", "cb"),
        P("ra", "cb"),
        P("cb", "ra"),
        P("ra"),
        P("ra", "cb"),
        P("ra", "cb"),
        P("cb", "ra"),
    )
    return jax.shard_map(
        per_device, mesh=mesh, in_specs=placed, out_specs=P("grp", "ra"), check_vma=False
    )
```

time: 89.2 us -> 79.6 us (0.89)
  waiting for transfers between devices: 71.6 us -> 31.8 us
  starting transfers between devices: 10.3 us -> 37.2 us
  matrix products: 2.27 us -> 4.48 us
  local copies, waits for them, and re-layouts: 0.25 us -> 1.49 us
    ppermute x12 -> x24, waiting for transfers between devices: 71.6 us -> 31.8 us  [per_device(): lax.ppermute(payload, axis, [(i, i ^ bit) for i in range(lax.axis_size(ax...]
    ppermute x12 -> x24, starting transfers between devices: 10.3 us -> 37.2 us  [per_device(): lax.ppermute(payload, axis, [(i, i ^ bit) for i in range(lax.axis_size(ax...]
    select_n x3 -> x5, other arithmetic: 1.87 us -> 0.09 us  [local_order(): y = jnp.where(me & bit != 0, jnp.flip(y, dim), y)]
    slice x4 -> x9, local copies, waits for them, and re-layouts: 0.13 us -> 1.17 us  [the longest x1 1.03 us: per_device(): tokens[c * rows:(c + 1) * rows]]
  transfers between devices with their start and end apart: 12 -> 24, of which waited for: 12 -> 17; matrix products, arithmetic and copies ran while one was open for 0% -> 6% of each run, Pallas kernels for 0% -> 0%
where the time goes in v2:
time: 79.6 us; the launch traced here: 79.5 us
  starting transfers between devices  37.2 us (47%)
  waiting for transfers between devices  31.8 us (40%)
  matrix products  4.48 us (6%)
  other arithmetic  4.03 us (5%)
  local copies, waits for them, and re-layouts  1.49 us (2%)
    ppermute x24, starting transfers between devices, per_device(): lax.ppermute(payload, axis, [(i, i ^ bit) for i in range(lax.axis_size(ax...  37.2 us
    ppermute x24, waiting for transfers between devices, per_device(): lax.ppermute(payload, axis, [(i, i ^ bit) for i in range(lax.axis_size(ax...  31.8 us
  transfers between devices with their start and end apart: 24, of which 17 were waited for; matrix products, arithmetic and copies ran while one was open for 6% of the time, Pallas kernels for 0%

profile of v2, /device:TPU:0, one launch (start us, length us, event | category | flops | bytes accessed | tf_op | source)
XLA Modules:
  0.0 79.5 jit_solution(17952245473127662116)
XLA Ops:
  3.2 3.1 %collective-permute-start = (bf16[32,2944]{1,0:T(8,128)(2,1)S(1)}, bf16[32,2944]{1,0:T(8,128)(2,1)S(1)}, u32[]{:S(2)}, u32[]{:S(2)}) collective-permute-start(bf16[32,2944]{1,0:T(8,128)(2,1)S(1)} %slice.267), channel_id=1, source_target_pairs={{0,4},{4,0},{8,12},{12,8},{1,5},{5,1},{9,13},{13,9},{2,6},{6,2},{1... | collective-permute-start | bytes 565256 | tf_op jit(solution)/shard_map/ppermute | solution.py:76
  7.4 4.5 %collective-permute-done = bf16[32,2944]{1,0:T(8,128)(2,1)S(1)} collective-permute-done((bf16[32,2944]{1,0:T(8,128)(2,1)S(1)}, bf16[32,2944]{1,0:T(8,128)(2,1)S(1)}, u32[]{:S(2)}, u32[]{:S(2)}) %collective-permute-start) | collective-permute-done | bytes 188448 | tf_op jit(solution)/shard_map/ppermute | solution.py:76
  12.0 3.1 %collective-permute-start.1 = (bf16[16,2944]{1,0:T(8,128)(2,1)S(1)}, bf16[16,2944]{1,0:T(8,128)(2,1)S(1)}, u32[]{:S(2)}, u32[]{:S(2)}) collective-permute-start(bf16[16,2944]{1,0:T(8,128)(2,1)S(1)} %slice.271), channel_id=1, source_target_pairs={{0,8},{4,12},{8,0},{12,4},{1,9},{5,13},{9,1},{13,5},{2,10},{6,14},... | collective-permute-start | bytes 282632 | tf_op jit(solution)/shard_map/ppermute | solution.py:76
  16.2 2.8 %collective-permute-start.4 = (bf16[16,2944]{1,0:T(8,128)(2,1)S(1)}, bf16[16,2944]{1,0:T(8,128)(2,1)S(1)}, u32[]{:S(2)}, u32[]{:S(2)}) collective-permute-start(bf16[16,2944]{1,0:T(8,128)(2,1)S(1)} %slice.270), channel_id=1, source_target_pairs={{0,8},{4,12},{8,0},{12,4},{1,9},{5,13},{9,1},{13,5},{2,10},{6,14},... | collective-permute-start | bytes 282632 | tf_op jit(solution)/shard_map/ppermute | solution.py:76
  19.0 1.5 %collective-permute-done.1 = bf16[16,2944]{1,0:T(8,128)(2,1)S(1)} collective-permute-done((bf16[16,2944]{1,0:T(8,128)(2,1)S(1)}, bf16[16,2944]{1,0:T(8,128)(2,1)S(1)}, u32[]{:S(2)}, u32[]{:S(2)}) %collective-permute-start.1) | collective-permute-done | bytes 94240 | tf_op jit(solution)/shard_map/ppermute | solution.py:76
  21.1 3.0 %collective-permute-done.4 = bf16[16,2944]{1,0:T(8,128)(2,1)S(1)} collective-permute-done((bf16[16,2944]{1,0:T(8,128)(2,1)S(1)}, bf16[16,2944]{1,0:T(8,128)(2,1)S(1)}, u32[]{:S(2)}, u32[]{:S(2)}) %collective-permute-start.4) | collective-permute-done | bytes 94240 | tf_op jit(solution)/shard_map/ppermute | solution.py:76
  25.8 3.3 %collective-permute-start.5 = (bf16[32,1408]{1,0:T(8,128)(2,1)S(1)}, bf16[32,1408]{1,0:T(8,128)(2,1)S(1)}, u32[]{:S(2)}, u32[]{:S(2)}) collective-permute-start(bf16[32,1408]{1,0:T(8,128)(2,1)S(1)} %pad_maximum_fusion.5), channel_id=1, source_target_pairs={{0,4},{4,0},{8,12},{12,8},{1,5},{5,1},{9,13},{13,9},{2,6},{6,2},{1... | collective-permute-start | bytes 270344 | tf_op jit(solution)/shard_map/ppermute | solution.py:76
  29.6 2.7 %collective-permute-start.8 = (bf16[32,1408]{1,0:T(8,128)(2,1)S(1)}, bf16[32,1408]{1,0:T(8,128)(2,1)S(1)}, u32[]{:S(2)}, u32[]{:S(2)}) collective-permute-start(bf16[32,1408]{1,0:T(8,128)(2,1)S(1)} %pad_maximum_fusion.6), channel_id=1, source_target_pairs={{0,4},{4,0},{8,12},{12,8},{1,5},{5,1},{9,13},{13,9},{2,6},{6,2},{1... | collective-permute-start | bytes 270344 | tf_op jit(solution)/shard_map/ppermute | solution.py:76
  32.7 2.0 %collective-permute-done.8 = bf16[32,1408]{1,0:T(8,128)(2,1)S(1)} collective-permute-done((bf16[32,1408]{1,0:T(8,128)(2,1)S(1)}, bf16[32,1408]{1,0:T(8,128)(2,1)S(1)}, u32[]{:S(2)}, u32[]{:S(2)}) %collective-permute-start.8) | collective-permute-done | bytes 90144 | tf_op jit(solution)/shard_map/ppermute | solution.py:76
  35.3 1.6 %collective-permute-start.9 = (bf16[64,512]{1,0:T(8,128)(2,1)S(1)}, bf16[64,512]{1,0:T(8,128)(2,1)S(1)}, u32[]{:S(2)}, u32[]{:S(2)}) collective-permute-start(bf16[64,512]{1,0:T(8,128)(2,1)S(1)} %fusion.40), channel_id=1, source_target_pairs={{0,2},{1,3},{2,0},{3,1},{4,6},{5,7},{6,4},{7,5},{8,10},{9,11},{10,... | collective-permute-start | bytes 196616 | tf_op jit(solution)/shard_map/ppermute | solution.py:76
  38.1 1.9 %collective-permute-done.9 = bf16[64,512]{1,0:T(8,128)(2,1)S(1)} collective-permute-done((bf16[64,512]{1,0:T(8,128)(2,1)S(1)}, bf16[64,512]{1,0:T(8,128)(2,1)S(1)}, u32[]{:S(2)}, u32[]{:S(2)}) %collective-permute-start.9) | collective-permute-done | bytes 65568 | tf_op jit(solution)/shard_map/ppermute | solution.py:76
  42.4 2.1 %collective-permute-start.11 = (bf16[32,2944]{1,0:T(8,128)(2,1)S(1)}, bf16[32,2944]{1,0:T(8,128)(2,1)S(1)}, u32[]{:S(2)}, u32[]{:S(2)}) collective-permute-start(bf16[32,2944]{1,0:T(8,128)(2,1)S(1)} %slice.265), channel_id=1, source_target_pairs={{0,4},{4,0},{8,12},{12,8},{1,5},{5,1},{9,13},{13,9},{2,6},{6,2},{1... | collective-permute-start | bytes 565256 | tf_op jit(solution)/shard_map/ppermute | solution.py:76
  44.6 5.4 %collective-permute-done.11 = bf16[32,2944]{1,0:T(8,128)(2,1)S(1)} collective-permute-done((bf16[32,2944]{1,0:T(8,128)(2,1)S(1)}, bf16[32,2944]{1,0:T(8,128)(2,1)S(1)}, u32[]{:S(2)}, u32[]{:S(2)}) %collective-permute-start.11) | collective-permute-done | bytes 188448 | tf_op jit(solution)/shard_map/ppermute | solution.py:76
  50.1 2.2 %collective-permute-start.13 = (bf16[16,2944]{1,0:T(8,128)(2,1)S(1)}, bf16[16,2944]{1,0:T(8,128)(2,1)S(1)}, u32[]{:S(2)}, u32[]{:S(2)}) collective-permute-start(bf16[16,2944]{1,0:T(8,128)(2,1)S(1)} %slice.269), channel_id=1, source_target_pairs={{0,8},{4,12},{8,0},{12,4},{1,9},{5,13},{9,1},{13,5},{2,10},{6,14},... | collective-permute-start | bytes 282632 | tf_op jit(solution)/shard_map/ppermute | solution.py:76
  52.3 1.6 %collective-permute-done.14 = bf16[32,2944]{1,0:T(8,128)(2,1)S(1)} collective-permute-done((bf16[32,2944]{1,0:T(8,128)(2,1)S(1)}, bf16[32,2944]{1,0:T(8,128)(2,1)S(1)}, u32[]{:S(2)}, u32[]{:S(2)}) %collective-permute-start.14) | collective-permute-done | bytes 188448 | tf_op jit(solution)/shard_map/ppermute | solution.py:76
  53.9 1.9 %collective-permute-start.16 = (bf16[16,2944]{1,0:T(8,128)(2,1)S(1)}, bf16[16,2944]{1,0:T(8,128)(2,1)S(1)}, u32[]{:S(2)}, u32[]{:S(2)}) collective-permute-start(bf16[16,2944]{1,0:T(8,128)(2,1)S(1)} %slice.268), channel_id=1, source_target_pairs={{0,8},{4,12},{8,0},{12,4},{1,9},{5,13},{9,1},{13,5},{2,10},{6,14},... | collective-permute-start | bytes 282632 | tf_op jit(solution)/shard_map/ppermute | solution.py:76
  56.1 3.0 %collective-permute-start.15 = (bf16[16,1408]{1,0:T(8,128)(2,1)S(1)}, bf16[16,1408]{1,0:T(8,128)(2,1)S(1)}, u32[]{:S(2)}, u32[]{:S(2)}) collective-permute-start(bf16[16,1408]{1,0:T(8,128)(2,1)S(1)} %fusion.47), channel_id=1, source_target_pairs={{0,8},{4,12},{8,0},{12,4},{1,9},{5,13},{9,1},{13,5},{2,10},{6,14},... | collective-permute-start | bytes 135176 | tf_op jit(solution)/shard_map/ppermute | solution.py:76
  59.1 2.8 %collective-permute-done.16 = bf16[16,2944]{1,0:T(8,128)(2,1)S(1)} collective-permute-done((bf16[16,2944]{1,0:T(8,128)(2,1)S(1)}, bf16[16,2944]{1,0:T(8,128)(2,1)S(1)}, u32[]{:S(2)}, u32[]{:S(2)}) %collective-permute-start.16) | collective-permute-done | bytes 94240 | tf_op jit(solution)/shard_map/ppermute | solution.py:76
  62.6 3.7 %collective-permute-start.17 = (bf16[32,1408]{1,0:T(8,128)(2,1)S(1)}, bf16[32,1408]{1,0:T(8,128)(2,1)S(1)}, u32[]{:S(2)}, u32[]{:S(2)}) collective-permute-start(bf16[32,1408]{1,0:T(8,128)(2,1)S(1)} %pad_maximum_fusion.7), channel_id=1, source_target_pairs={{0,4},{4,0},{8,12},{12,8},{1,5},{5,1},{9,13},{13,9},{2,6},{6,2},{1... | collective-permute-start | bytes 270344 | tf_op jit(solution)/shard_map/ppermute | solution.py:76
  67.3 2.4 %collective-permute-start.20 = (bf16[32,1408]{1,0:T(8,128)(2,1)S(1)}, bf16[32,1408]{1,0:T(8,128)(2,1)S(1)}, u32[]{:S(2)}, u32[]{:S(2)}) collective-permute-start(bf16[32,1408]{1,0:T(8,128)(2,1)S(1)} %pad_maximum_fusion.8), channel_id=1, source_target_pairs={{0,4},{4,0},{8,12},{12,8},{1,5},{5,1},{9,13},{13,9},{2,6},{6,2},{1... | collective-permute-start | bytes 270344 | tf_op jit(solution)/shard_map/ppermute | solution.py:76
  70.1 2.0 %collective-permute-done.20 = bf16[32,1408]{1,0:T(8,128)(2,1)S(1)} collective-permute-done((bf16[32,1408]{1,0:T(8,128)(2,1)S(1)}, bf16[32,1408]{1,0:T(8,128)(2,1)S(1)}, u32[]{:S(2)}, u32[]{:S(2)}) %collective-permute-start.20) | collective-permute-done | bytes 90144 | tf_op jit(solution)/shard_map/ppermute | solution.py:76
  72.6 1.7 %collective-permute-start.21 = (bf16[64,512]{1,0:T(8,128)(2,1)S(1)}, bf16[64,512]{1,0:T(8,128)(2,1)S(1)}, u32[]{:S(2)}, u32[]{:S(2)}) collective-permute-start(bf16[64,512]{1,0:T(8,128)(2,1)S(1)} %fusion.42), channel_id=1, source_target_pairs={{0,2},{1,3},{2,0},{3,1},{4,6},{5,7},{6,4},{7,5},{8,10},{9,11},{10,... | collective-permute-start | bytes 196616 | tf_op jit(solution)/shard_map/ppermute | solution.py:76
  75.6 1.6 %collective-permute-done.21 = bf16[64,512]{1,0:T(8,128)(2,1)S(1)} collective-permute-done((bf16[64,512]{1,0:T(8,128)(2,1)S(1)}, bf16[64,512]{1,0:T(8,128)(2,1)S(1)}, u32[]{:S(2)}, u32[]{:S(2)}) %collective-permute-start.21) | collective-permute-done | bytes 65568 | tf_op jit(solution)/shard_map/ppermute | solution.py:76
  77.2 1.5 %collective-permute-done.23 = bf16[64,512]{1,0:T(8,128)(2,1)S(1)} collective-permute-done((bf16[64,512]{1,0:T(8,128)(2,1)S(1)}, bf16[64,512]{1,0:T(8,128)(2,1)S(1)}, u32[]{:S(2)}, u32[]{:S(2)}) %collective-permute-start.23) | collective-permute-done | bytes 65568 | tf_op jit(solution)/shard_map/ppermute | solution.py:76
  (112 shorter events, 17.7 us)
Async XLA Ops:
  3.2 8.7 %collective-permute-start = (bf16[32,2944]{1,0:T(8,128)(2,1)S(1)}, bf16[32,2944]{1,0:T(8,128)(2,1)S(1)}, u32[]{:S(2)}, u32[]{:S(2)}) collective-permute-start(bf16[32,2944]{1,0:T(8,128)(2,1)S(1)} %slice.267), channel_id=1, source_target_pairs={{0,4},{4,0},{8,12},{12,8},{1,5},{5,1},{9,13},{13,9},{2,6},{6,2},{1... | collective-permute-start | bytes 565256 | tf_op jit(solution)/shard_map/ppermute | solution.py:76
  7.2 8.9 %collective-permute-start.2 = (bf16[32,2944]{1,0:T(8,128)(2,1)S(1)}, bf16[32,2944]{1,0:T(8,128)(2,1)S(1)}, u32[]{:S(2)}, u32[]{:S(2)}) collective-permute-start(bf16[32,2944]{1,0:T(8,128)(2,1)S(1)} %slice.266), channel_id=1, source_target_pairs={{0,4},{4,0},{8,12},{12,8},{1,5},{5,1},{9,13},{13,9},{2,6},{6,2},{1... | collective-permute-start | bytes 565256 | tf_op jit(solution)/shard_map/ppermute | solution.py:76
  12.0 8.5 %collective-permute-start.1 = (bf16[16,2944]{1,0:T(8,128)(2,1)S(1)}, bf16[16,2944]{1,0:T(8,128)(2,1)S(1)}, u32[]{:S(2)}, u32[]{:S(2)}) collective-permute-start(bf16[16,2944]{1,0:T(8,128)(2,1)S(1)} %slice.271), channel_id=1, source_target_pairs={{0,8},{4,12},{8,0},{12,4},{1,9},{5,13},{9,1},{13,5},{2,10},{6,14},... | collective-permute-start | bytes 282632 | tf_op jit(solution)/shard_map/ppermute | solution.py:76
  16.2 8.0 %collective-permute-start.4 = (bf16[16,2944]{1,0:T(8,128)(2,1)S(1)}, bf16[16,2944]{1,0:T(8,128)(2,1)S(1)}, u32[]{:S(2)}, u32[]{:S(2)}) collective-permute-start(bf16[16,2944]{1,0:T(8,128)(2,1)S(1)} %slice.270), channel_id=1, source_target_pairs={{0,8},{4,12},{8,0},{12,4},{1,9},{5,13},{9,1},{13,5},{2,10},{6,14},... | collective-permute-start | bytes 282632 | tf_op jit(solution)/shard_map/ppermute | solution.py:76
  20.8 5.0 %collective-permute-start.3 = (bf16[16,1408]{1,0:T(8,128)(2,1)S(1)}, bf16[16,1408]{1,0:T(8,128)(2,1)S(1)}, u32[]{:S(2)}, u32[]{:S(2)}) collective-permute-start(bf16[16,1408]{1,0:T(8,128)(2,1)S(1)} %fusion.51), channel_id=1, source_target_pairs={{0,8},{4,12},{8,0},{12,4},{1,9},{5,13},{9,1},{13,5},{2,10},{6,14},... | collective-permute-start | bytes 135176 | tf_op jit(solution)/shard_map/ppermute | solution.py:76
  24.5 5.0 %collective-permute-start.6 = (bf16[16,1408]{1,0:T(8,128)(2,1)S(1)}, bf16[16,1408]{1,0:T(8,128)(2,1)S(1)}, u32[]{:S(2)}, u32[]{:S(2)}) collective-permute-start(bf16[16,1408]{1,0:T(8,128)(2,1)S(1)} %fusion.49), channel_id=1, source_target_pairs={{0,8},{4,12},{8,0},{12,4},{1,9},{5,13},{9,1},{13,5},{2,10},{6,14},... | collective-permute-start | bytes 135176 | tf_op jit(solution)/shard_map/ppermute | solution.py:76
  25.8 6.5 %collective-permute-start.5 = (bf16[32,1408]{1,0:T(8,128)(2,1)S(1)}, bf16[32,1408]{1,0:T(8,128)(2,1)S(1)}, u32[]{:S(2)}, u32[]{:S(2)}) collective-permute-start(bf16[32,1408]{1,0:T(8,128)(2,1)S(1)} %pad_maximum_fusion.5), channel_id=1, source_target_pairs={{0,4},{4,0},{8,12},{12,8},{1,5},{5,1},{9,13},{13,9},{2,6},{6,2},{1... | collective-permute-start | bytes 270344 | tf_op jit(solution)/shard_map/ppermute | solution.py:76
  29.6 5.2 %collective-permute-start.8 = (bf16[32,1408]{1,0:T(8,128)(2,1)S(1)}, bf16[32,1408]{1,0:T(8,128)(2,1)S(1)}, u32[]{:S(2)}, u32[]{:S(2)}) collective-permute-start(bf16[32,1408]{1,0:T(8,128)(2,1)S(1)} %pad_maximum_fusion.6), channel_id=1, source_target_pairs={{0,4},{4,0},{8,12},{12,8},{1,5},{5,1},{9,13},{13,9},{2,6},{6,2},{1... | collective-permute-start | bytes 270344 | tf_op jit(solution)/shard_map/ppermute | solution.py:76
  32.7 2.6 %collective-permute-start.7 = (bf16[64,512]{1,0:T(8,128)(2,1)S(1)}, bf16[64,512]{1,0:T(8,128)(2,1)S(1)}, u32[]{:S(2)}, u32[]{:S(2)}) collective-permute-start(bf16[64,512]{1,0:T(8,128)(2,1)S(1)} %get-tuple-element.35), channel_id=1, source_target_pairs={{0,1},{1,0},{2,3},{3,2},{4,5},{5,4},{6,7},{7,6},{8,9},{9,8},{10,11... | collective-permute-start | bytes 196616 | tf_op jit(solution)/shard_map/ppermute | solution.py:76
  35.2 1.7 %collective-permute-start.10 = (bf16[64,512]{1,0:T(8,128)(2,1)S(1)}, bf16[64,512]{1,0:T(8,128)(2,1)S(1)}, u32[]{:S(2)}, u32[]{:S(2)}) collective-permute-start(bf16[64,512]{1,0:T(8,128)(2,1)S(1)} %get-tuple-element.36), channel_id=1, source_target_pairs={{0,1},{1,0},{2,3},{3,2},{4,5},{5,4},{6,7},{7,6},{8,9},{9,8},{10,11... | collective-permute-start | bytes 196616 | tf_op jit(solution)/shard_map/ppermute | solution.py:76
  35.3 4.7 %collective-permute-start.9 = (bf16[64,512]{1,0:T(8,128)(2,1)S(1)}, bf16[64,512]{1,0:T(8,128)(2,1)S(1)}, u32[]{:S(2)}, u32[]{:S(2)}) collective-permute-start(bf16[64,512]{1,0:T(8,128)(2,1)S(1)} %fusion.40), channel_id=1, source_target_pairs={{0,2},{1,3},{2,0},{3,1},{4,6},{5,7},{6,4},{7,5},{8,10},{9,11},{10,... | collective-permute-start | bytes 196616 | tf_op jit(solution)/shard_map/ppermute | solution.py:76
  36.8 4.4 %collective-permute-start.12 = (bf16[64,512]{1,0:T(8,128)(2,1)S(1)}, bf16[64,512]{1,0:T(8,128)(2,1)S(1)}, u32[]{:S(2)}, u32[]{:S(2)}) collective-permute-start(bf16[64,512]{1,0:T(8,128)(2,1)S(1)} %fusion.41), channel_id=1, source_target_pairs={{0,2},{1,3},{2,0},{3,1},{4,6},{5,7},{6,4},{7,5},{8,10},{9,11},{10,... | collective-permute-start | bytes 196616 | tf_op jit(solution)/shard_map/ppermute | solution.py:76
  42.4 7.7 %collective-permute-start.11 = (bf16[32,2944]{1,0:T(8,128)(2,1)S(1)}, bf16[32,2944]{1,0:T(8,128)(2,1)S(1)}, u32[]{:S(2)}, u32[]{:S(2)}) collective-permute-start(bf16[32,2944]{1,0:T(8,128)(2,1)S(1)} %slice.265), channel_id=1, source_target_pairs={{0,4},{4,0},{8,12},{12,8},{1,5},{5,1},{9,13},{13,9},{2,6},{6,2},{1... | collective-permute-start | bytes 565256 | tf_op jit(solution)/shard_map/ppermute | solution.py:76
  44.5 9.3 %collective-permute-start.14 = (bf16[32,2944]{1,0:T(8,128)(2,1)S(1)}, bf16[32,2944]{1,0:T(8,128)(2,1)S(1)}, u32[]{:S(2)}, u32[]{:S(2)}) collective-permute-start(bf16[32,2944]{1,0:T(8,128)(2,1)S(1)} %slice.264), channel_id=1, source_target_pairs={{0,4},{4,0},{8,12},{12,8},{1,5},{5,1},{9,13},{13,9},{2,6},{6,2},{1... | collective-permute-start | bytes 565256 | tf_op jit(solution)/shard_map/ppermute | solution.py:76
  50.1 5.7 %collective-permute-start.13 = (bf16[16,2944]{1,0:T(8,128)(2,1)S(1)}, bf16[16,2944]{1,0:T(8,128)(2,1)S(1)}, u32[]{:S(2)}, u32[]{:S(2)}) collective-permute-start(bf16[16,2944]{1,0:T(8,128)(2,1)S(1)} %slice.269), channel_id=1, source_target_pairs={{0,8},{4,12},{8,0},{12,4},{1,9},{5,13},{9,1},{13,5},{2,10},{6,14},... | collective-permute-start | bytes 282632 | tf_op jit(solution)/shard_map/ppermute | solution.py:76
  53.9 8.0 %collective-permute-start.16 = (bf16[16,2944]{1,0:T(8,128)(2,1)S(1)}, bf16[16,2944]{1,0:T(8,128)(2,1)S(1)}, u32[]{:S(2)}, u32[]{:S(2)}) collective-permute-start(bf16[16,2944]{1,0:T(8,128)(2,1)S(1)} %slice.268), channel_id=1, source_target_pairs={{0,8},{4,12},{8,0},{12,4},{1,9},{5,13},{9,1},{13,5},{2,10},{6,14},... | collective-permute-start | bytes 282632 | tf_op jit(solution)/shard_map/ppermute | solution.py:76
  56.1 6.5 %collective-permute-start.15 = (bf16[16,1408]{1,0:T(8,128)(2,1)S(1)}, bf16[16,1408]{1,0:T(8,128)(2,1)S(1)}, u32[]{:S(2)}, u32[]{:S(2)}) collective-permute-start(bf16[16,1408]{1,0:T(8,128)(2,1)S(1)} %fusion.47), channel_id=1, source_target_pairs={{0,8},{4,12},{8,0},{12,4},{1,9},{5,13},{9,1},{13,5},{2,10},{6,14},... | collective-permute-start | bytes 135176 | tf_op jit(solution)/shard_map/ppermute | solution.py:76
  62.3 5.0 %collective-permute-start.18 = (bf16[16,1408]{1,0:T(8,128)(2,1)S(1)}, bf16[16,1408]{1,0:T(8,128)(2,1)S(1)}, u32[]{:S(2)}, u32[]{:S(2)}) collective-permute-start(bf16[16,1408]{1,0:T(8,128)(2,1)S(1)} %fusion.45), channel_id=1, source_target_pairs={{0,8},{4,12},{8,0},{12,4},{1,9},{5,13},{9,1},{13,5},{2,10},{6,14},... | collective-permute-start | bytes 135176 | tf_op jit(solution)/shard_map/ppermute | solution.py:76
  62.6 7.1 %collective-permute-start.17 = (bf16[32,1408]{1,0:T(8,128)(2,1)S(1)}, bf16[32,1408]{1,0:T(8,128)(2,1)S(1)}, u32[]{:S(2)}, u32[]{:S(2)}) collective-permute-start(bf16[32,1408]{1,0:T(8,128)(2,1)S(1)} %pad_maximum_fusion.7), channel_id=1, source_target_pairs={{0,4},{4,0},{8,12},{12,8},{1,5},{5,1},{9,13},{13,9},{2,6},{6,2},{1... | collective-permute-start | bytes 270344 | tf_op jit(solution)/shard_map/ppermute | solution.py:76
  67.3 4.9 %collective-permute-start.20 = (bf16[32,1408]{1,0:T(8,128)(2,1)S(1)}, bf16[32,1408]{1,0:T(8,128)(2,1)S(1)}, u32[]{:S(2)}, u32[]{:S(2)}) collective-permute-start(bf16[32,1408]{1,0:T(8,128)(2,1)S(1)} %pad_maximum_fusion.8), channel_id=1, source_target_pairs={{0,4},{4,0},{8,12},{12,8},{1,5},{5,1},{9,13},{13,9},{2,6},{6,2},{1... | collective-permute-start | bytes 270344 | tf_op jit(solution)/shard_map/ppermute | solution.py:76
  70.0 2.6 %collective-permute-start.19 = (bf16[64,512]{1,0:T(8,128)(2,1)S(1)}, bf16[64,512]{1,0:T(8,128)(2,1)S(1)}, u32[]{:S(2)}, u32[]{:S(2)}) collective-permute-start(bf16[64,512]{1,0:T(8,128)(2,1)S(1)} %get-tuple-element.47), channel_id=1, source_target_pairs={{0,1},{1,0},{2,3},{3,2},{4,5},{5,4},{6,7},{7,6},{8,9},{9,8},{10,11... | collective-permute-start | bytes 196616 | tf_op jit(solution)/shard_map/ppermute | solution.py:76
  72.5 1.8 %collective-permute-start.22 = (bf16[64,512]{1,0:T(8,128)(2,1)S(1)}, bf16[64,512]{1,0:T(8,128)(2,1)S(1)}, u32[]{:S(2)}, u32[]{:S(2)}) collective-permute-start(bf16[64,512]{1,0:T(8,128)(2,1)S(1)} %get-tuple-element.48), channel_id=1, source_target_pairs={{0,1},{1,0},{2,3},{3,2},{4,5},{5,4},{6,7},{7,6},{8,9},{9,8},{10,11... | collective-permute-start | bytes 196616 | tf_op jit(solution)/shard_map/ppermute | solution.py:76
  72.6 4.5 %collective-permute-start.21 = (bf16[64,512]{1,0:T(8,128)(2,1)S(1)}, bf16[64,512]{1,0:T(8,128)(2,1)S(1)}, u32[]{:S(2)}, u32[]{:S(2)}) collective-permute-start(bf16[64,512]{1,0:T(8,128)(2,1)S(1)} %fusion.42), channel_id=1, source_target_pairs={{0,2},{1,3},{2,0},{3,1},{4,6},{5,7},{6,4},{7,5},{8,10},{9,11},{10,... | collective-permute-start | bytes 196616 | tf_op jit(solution)/shard_map/ppermute | solution.py:76
  74.4 4.3 %collective-permute-start.23 = (bf16[64,512]{1,0:T(8,128)(2,1)S(1)}, bf16[64,512]{1,0:T(8,128)(2,1)S(1)}, u32[]{:S(2)}, u32[]{:S(2)}) collective-permute-start(bf16[64,512]{1,0:T(8,128)(2,1)S(1)} %fusion.43), channel_id=1, source_target_pairs={{0,2},{1,3},{2,0},{3,1},{4,6},{5,7},{6,4},{7,5},{8,10},{9,11},{10,... | collective-permute-start | bytes 196616 | tf_op jit(solution)/shard_map/ppermute | solution.py:76
  (7 other events, 58.2 us)
